TPU v7x, 32 devices: a whole 2x2x4 slice. The times are simulated.
32 devices in a mesh: sp: 8 (over z, y), tp: 4 (over x, core).
Axes of the slice: x: 2, y: 2, z: 4, core: 2. Of those that a mesh axis runs over, the one named last changes fastest.
Arguments:
- tokens: bfloat16 [1280, 2048], P('sp'), may hold values from -8 to 8
- query_weight: bfloat16 [2048, 2048], P('sp', 'tp'), may hold values from -0.5 to 0.5
- key_weight: bfloat16 [2048, 2048], P('sp', 'tp'), may hold values from -0.5 to 0.5
- value_weight: bfloat16 [2048, 2048], P('sp', 'tp'), may hold values from -0.125 to 0.125
- out_weight: bfloat16 [2048, 2048], P('tp', 'sp'), may hold values from -0.125 to 0.125
- mix_lambda: float32 [16], P('tp'), may hold values from 0.3 to 0.8
- head_gain: float32 [128], replicated, may hold values from 0.1 to 1.9
Outputs:
- attended: bfloat16 [1280, 2048], P('sp')
All inputs are finite; a program needn't handle non-finite values.
Results may differ from a plain program's by a relative error of at most 0.018.
The roundings to bfloat16 on the way count: a program that leaves them out, or rounds other values in their place, can miss the bound.
Values may be sent and summed in bfloat16 or wider, within the bound.
A program may use at most 192 MiB of HBM per device.

v0:
```python
import functools

import jax
import jax.numpy as jnp
from jax import lax
from jax.experimental import pallas as pl
from jax.experimental.pallas import tpu as pltpu
from jax.sharding import PartitionSpec as P

MESH = pl.DeviceIdType.MESH
Q, K, V = 0, 1, 2
PLAN = (
    "t0", "yv", "Wv1", "Wk3", "t10", "fv1", "t11", "Wv3", "Wv2", "Wk1", "yq", "Wq3", "yk", "fk3",
    "t20", "fv2", "m11", "m20", "fv3", "m10", "Wk2", "fk1", "Wq1", "t21", "hv", "e1", "fq3", "m21",
    "Wq2", "fk2", "fq1", "O", "t31", "hk", "t30", "b0", "fq2", "m31", "e2", "b2", "b1", "m30", "e3",
    "b3", "gq", "o1", "hq", "dq", "a0", "a3", "a2", "a1", "r0", "r3", "o2", "r1", "r2", "P00",
    "S00", "H", "P10", "S10", "o3", "P11", "X00", "S11", "X10", "P01", "S01", "X11", "F0", "F1",
    "X01", "Z",
)


def kernel(
    n, parts, heads, chunks,
    tok, wq, wk, wv, wo_in, lam_in, gain_in, out,
    x, wown, w, acc, qb, kv, wo, ho_out, ho, part_out, part_in, sum_out, sum_in, staged, gain, lam,
    local_sem, sent, xz_recv, xx_recv, xe_recv, wz_recv, wy_recv, kv_recv, wo_recv, ho_recv,
    hof_recv, p_recv, s_recv, f_recv, d_recv,
):
    groups = n // heads
    s, t = lax.axis_index("sp"), lax.axis_index("tp")
    h, r = lax.div(s, groups), lax.rem(s, groups)
    rows, width = tok.shape
    depth = wq.shape[0]
    vdim = gain.shape[-1]
    seg = width // parts
    ocols = wo_in.shape[1]
    bits = [1 << i for i in range(parts.bit_length() - 1)]
    by_source = depth % 128 == 0
    low = lax.rem(t, 2)
    pairs = heads // 2
    chunk = rows // chunks

    def at_sp(index):
        return (index, t)

    def at_tp(index):
        return (s, index)

    def flip(index, bit):
        return index + bit - 2 * bit * lax.rem(lax.div(index, bit), 2)

    def ds(index, size):
        return pl.ds(pl.multiple_of(index * size, size), size)

    (TOKENS_Z, WEIGHTS_Z, WEIGHTS_Y, SPREAD, KEYS_Y, OUT_Z, HEADS_Z, HEADS_Y,
     PARTS, SUMS, RESULTS_Y, RESULTS) = range(12)

    def send(src, dst, kind, recv_sem, device, cond=None):
        copy = pltpu.make_async_remote_copy(
            src_ref=src, dst_ref=dst, send_sem=sent.at[kind], recv_sem=recv_sem,
            device_id=device, device_id_type=MESH,
        )
        if cond is None:
            copy.start()
        else:
            pl.when(cond)(copy.start)

    def arrived(ref, sem):
        pltpu.make_async_copy(ref, ref, sem).wait()

    barrier = pltpu.get_barrier_semaphore()
    for d in range(1, heads):
        pl.semaphore_signal(
            barrier, inc=1, device_id=at_sp(lax.rem(h + d, heads) * groups + r), device_id_type=MESH
        )
    for d in range(1, groups):
        pl.semaphore_signal(
            barrier, inc=1, device_id=at_sp(h * groups + lax.rem(r + d, groups)), device_id_type=MESH
        )
    for bit in bits:
        pl.semaphore_signal(barrier, inc=1, device_id=at_tp(flip(t, bit)), device_id_type=MESH)

    def x_at(block, part, c):
        return x.at[ds(block * chunks + c, chunk), ds(part, seg)]

    def w_at(block, i):
        return w.at[ds(block, depth), pl.ds(i * vdim, vdim)]

    right, left = at_sp(s + groups), at_sp(s - groups)
    can_right, can_left = h + 1 < heads, h > 0
    onward = ((right, can_right), (left, can_left))
    weights = (wq, wk, wv)
    peers = [at_sp(h * groups + lax.rem(r + e, groups)) for e in range(1, groups)]
    others = [lax.rem(r + e, groups) for e in range(1, groups)]

    loads = {"tok": pltpu.make_async_copy(tok, x.at[ds(h, rows), :], local_sem.at[0])}
    for i in (V, K, Q):
        loads["own", i] = pltpu.make_async_copy(weights[i], wown.at[i], local_sem.at[1 + i])
        loads["mine", i] = pltpu.make_async_copy(
            weights[i].at[:, ds(h, vdim)], w_at(s, i), local_sem.at[4 + i]
        )
    loads["out"] = pltpu.make_async_copy(wo_in, wo.at[h], local_sem.at[7])
    loads["lam"] = pltpu.make_async_copy(lam_in, lam, local_sem.at[8])
    loads["gain"] = pltpu.make_async_copy(gain_in, gain, local_sem.at[9])
    for copy in loads.values():
        copy.start()

    def loaded(key):
        if key in loads:
            loads.pop(key).wait()

    pl.semaphore_wait(barrier, heads + groups - 2 + len(bits))

    def send_tokens():
        loaded("tok")
        for c in range(chunks):
            for target, can in onward:
                send(x_at(h, t, c), x_at(h, t, c), TOKENS_Z, xz_recv.at[h, c], target, can)

    def send_own_weight(i):
        loaded(("mine", i))
        for peer in peers:
            send(w_at(s, i), w_at(s, i), WEIGHTS_Y, wy_recv.at[i], peer)

    def send_weight(i, d):
        loaded(("own", i))
        for owner, cond in ((h + d, h + d < heads), (h - d, h - d >= 0)):
            safe = jnp.where(cond, owner, h)
            send(wown.at[i, :, ds(safe, vdim)], w_at(s, i), WEIGHTS_Z, wz_recv.at[h, i],
                 at_sp(safe * groups + r), cond)

    spread = [(v, [b for b in reversed(bits) if v == 0 or b < (v & -v)]) for v in range(parts)]
    relays = [v for v, along in spread if v and along]
    leaves = parts - 1 - len(relays)

    def part_of(v):
        part = t
        for b in bits:
            if v & b:
                part = flip(part, b)
        return part

    def spread_sem(block, v, c):
        return xx_recv.at[block, relays.index(v), c] if v in relays else xe_recv.at[block]

    def pass_on(block, v, c, cond):
        piece = x_at(block, part_of(v), c)
        for b in spread[v][1]:
            send(piece, piece, SPREAD, spread_sem(block, v | b, c), at_tp(flip(t, b)), cond)

    def reach(k):
        if k == 0:
            return [(h, None, 0)]
        return [
            (jnp.where(have, block, h), have, side)
            for side, (block, have) in enumerate(((h - k, h - k >= 0), (h + k, h + k < heads)))
        ]

    def when(have, body):
        if have is None:
            body()
        else:
            pl.when(have)(body)

    def relay_tokens(k, c):
        for safe, have, side in reach(k):
            when(have, lambda safe=safe: arrived(x_at(safe, t, c), xz_recv.at[safe, c]))
            if k < heads - 1:
                target, can = onward[side]
                send(x_at(safe, t, c), x_at(safe, t, c), TOKENS_Z, xz_recv.at[safe, c], target,
                     jnp.logical_and(have, can))
            pass_on(safe, 0, c, have)

    def spread_tokens(k, c):
        for v in sorted(relays, reverse=True):
            for safe, have, _ in reach(k):
                when(have, lambda safe=safe: arrived(x_at(safe, part_of(v), c), spread_sem(safe, v, c)))
                pass_on(safe, v, c, have)

    def have_tokens(k):
        for safe, have, _ in reach(k):
            when(have, lambda safe=safe: arrived(x.at[ds(safe, rows), :leaves * seg], xe_recv.at[safe]))

    def forward_weight(i, d):
        for source_h, have, _ in reach(d):
            piece = w_at(source_h * groups + r, i)
            when(have, lambda piece=piece, source_h=source_h: arrived(piece, wz_recv.at[source_h, i]))
            for peer in peers:
                send(piece, piece, WEIGHTS_Y, wy_recv.at[i], peer, have)

    def have_weight(i):
        arrived(w.at[:(groups - 1) * heads * depth, pl.ds(i * vdim, vdim)], wy_recv.at[i])

    def begin_queries():
        loaded("tok")
        loaded(("mine", Q))
        if by_source:
            acc[...] = query_product(r)

    def query_product(group):
        total = None
        for k in range(heads):
            source = k * groups + group
            term = jnp.dot(x[:, ds(source, depth)], w[ds(source, depth), :vdim],
                           preferred_element_type=jnp.float32)
            total = term if total is None else total + term
        return total

    def finish_queries():
        if not by_source:
            full = jnp.dot(x[...], w[:, :vdim], preferred_element_type=jnp.float32)
        else:
            full = acc[...]
            for other in others:
                full = full + query_product(other)
        qb[...] = full.astype(jnp.bfloat16)

    def share_rows(k):
        loaded("tok")
        loaded(("mine", K))
        loaded(("mine", V))

        def body(block):
            mine = ds(block * groups + r, rows)
            kv[mine, :] = jnp.dot(
                x[ds(block, rows), :], w[:, vdim:], preferred_element_type=jnp.float32
            ).astype(jnp.bfloat16)
            for peer in peers:
                send(kv.at[mine, :], kv.at[mine, :], KEYS_Y, kv_recv.at[block], peer)

        for safe, have, _ in reach(k):
            when(have, lambda safe=safe: body(safe))

    def send_out_weight():
        loaded("out")
        for target, can in onward:
            send(wo.at[h], wo.at[h], OUT_Z, wo_recv.at[h], target, can)

    def relay_out_weight(k):
        for safe, have, side in reach(k):
            when(have, lambda safe=safe: arrived(wo.at[safe], wo_recv.at[safe]))
            if k < heads - 1:
                target, can = onward[side]
                send(wo.at[safe], wo.at[safe], OUT_Z, wo_recv.at[safe], target,
                     jnp.logical_and(have, can))

    lane = lax.broadcasted_iota(jnp.int32, (rows, vdim), 1)
    factor = (vdim // 2) ** (-0.5) * 1.4426950408889634
    seen = []

    def attend(k):
        for j in range(k + 1):
            if j not in seen:
                seen.append(j)
                arrived(kv.at[:(groups - 1) * rows, :], kv_recv.at[j])
        loaded("lam")
        loaded("gain")
        lam_here = jnp.float32(0.0)
        for j in range(heads):
            lam_here = jnp.where(h == j, lam[j], lam_here)
        extent = (k + 1) * groups * rows
        q_rows = qb[k * rows:(k + 1) * rows, :]
        keys = kv[:extent, :vdim]
        values = kv[:extent, vdim:]
        ahead = lax.broadcasted_iota(jnp.int32, (rows, extent), 1) - lax.broadcasted_iota(
            jnp.int32, (rows, extent), 0
        )
        visible = ahead <= (k * groups + r) * rows
        maps = []
        for c in range(2):
            picked = jnp.where((lane >= vdim // 2) == (c == 1), q_rows, jnp.zeros_like(q_rows))
            scores = lax.dot_general(
                picked, keys, (((1,), (1,)), ((), ())), preferred_element_type=jnp.float32
            )
            scores = jnp.where(visible, scores, -1e30)
            top = jnp.max(scores, axis=-1, keepdims=True)
            e = jnp.exp2((scores - top) * factor)
            total = jnp.sum(e, axis=-1, keepdims=True)
            mixed = jnp.dot(e.astype(jnp.bfloat16), values, preferred_element_type=jnp.float32)
            maps.append(mixed / total)
        mixture = maps[0] - lam_here * maps[1]
        normalized = (
            mixture
            * lax.rsqrt(jnp.mean(mixture * mixture, axis=-1, keepdims=True) + 1e-05)
            * gain[...]
        )
        ho_out[k] = normalized.astype(jnp.bfloat16)
        send(ho_out.at[k], ho.at[r, h], HEADS_Z, ho_recv.at[h], at_sp(k * groups + r), k != h)

        @pl.when(k == h)
        def _():
            ho[r, h] = ho_out[k]

    def forward_heads(d):
        for source, have, _ in reach(d):
            if d:
                when(have, lambda source=source: arrived(ho.at[r, source], ho_recv.at[source]))
            for peer in peers:
                send(ho.at[r, source], ho.at[r, source], HEADS_Y, hof_recv.at[0], peer, have)

    def have_heads():
        arrived(ho.at[:groups - 1], hof_recv.at[0])

    buddy = at_tp(flip(t, 1))
    members = [r] + others

    def column_block(p, which):
        return 2 * lax.rem(lax.div(h, 2) + p, pairs) + lax.rem(h + which, 2)

    def which_rows(later):
        return range(1, groups) if later else range(1)

    def partial_product(e, p, which):
        lhs = jnp.concatenate([ho[members[e], k] for k in range(heads)], axis=-1)
        return jnp.dot(lhs, wo[column_block(p, which)], preferred_element_type=jnp.float32)

    def project_theirs(later, p):
        for e in which_rows(later):
            j = e * pairs + p
            part_out[j] = partial_product(e, p, 1 - low).astype(jnp.bfloat16)
            send(part_out.at[j], part_in.at[j], PARTS, p_recv.at[j], buddy)

    def project_mine(later, p):
        for e in which_rows(later):
            j = e * pairs + p
            own = partial_product(e, p, low)
            arrived(part_in.at[j], p_recv.at[j])
            sum_out[0, j] = (own + part_in[j].astype(jnp.float32)).astype(jnp.bfloat16)
            send(sum_out.at[0, j], sum_in.at[0, j], SUMS, s_recv.at[0, j], at_tp(flip(t, bits[1])))

    def add_up(later, p):
        last = len(bits) - 1
        for e in which_rows(later):
            j = e * pairs + p
            for i in range(1, len(bits)):
                arrived(sum_in.at[i - 1, j], s_recv.at[i - 1, j])
                total = (
                    sum_out[i - 1, j].astype(jnp.float32) + sum_in[i - 1, j].astype(jnp.float32)
                ).astype(jnp.bfloat16)
                if i < last:
                    sum_out[i, j] = total
                    send(sum_out.at[i, j], sum_in.at[i, j], SUMS, s_recv.at[i, j],
                         at_tp(flip(t, bits[i + 1])))
            column = column_block(p, low) * groups + r
            if e == 0:
                staged[column] = total
                send(staged.at[column], staged.at[column], RESULTS, d_recv.at[0], buddy)
            else:
                sum_out[last, j] = total
                send(sum_out.at[last, j], staged.at[column], RESULTS_Y, f_recv.at[r, p], peers[e - 1])

    def finished(p):
        for other in others:
            column = column_block(p, low) * groups + other
            arrived(staged.at[column], f_recv.at[other, p])
            send(staged.at[column], staged.at[column], RESULTS, d_recv.at[0], buddy)

    def all_finished():
        arrived(part_in, d_recv.at[0])

    index = {"q": Q, "k": K, "v": V}
    run = {
        "t": lambda k, c=0: relay_tokens(int(k), int(c)) if int(k) else send_tokens(),
        "m": lambda k, c: spread_tokens(int(k), int(c)),
        "e": lambda k: have_tokens(int(k)),
        "y": lambda i: send_own_weight(index[i]),
        "W": lambda i, d: send_weight(index[i], int(d)),
        "f": lambda i, d: forward_weight(index[i], int(d)),
        "h": lambda i: have_weight(index[i]),
        "b": lambda k: share_rows(int(k)),
        "g": lambda i: begin_queries(),
        "d": lambda i: finish_queries(),
        "O": send_out_weight,
        "o": lambda k: relay_out_weight(int(k)),
        "a": lambda k: attend(int(k)),
        "r": lambda d: forward_heads(int(d)),
        "P": lambda e, p: project_theirs(int(e), int(p)),
        "S": lambda e, p: project_mine(int(e), int(p)),
        "H": have_heads,
        "X": lambda e, p: add_up(int(e), int(p)),
        "F": lambda p: finished(int(p)),
        "Z": all_finished,
    }
    for name in PLAN:
        run[name[0]](*name[1:])

    for column in range(n):
        out[:, column * ocols:(column + 1) * ocols] = staged[column]
    inner = jnp.logical_and(can_right, can_left)
    blocks = heads + 1
    out_rows = blocks * heads * vdim * ocols // width
    pl.when(inner)(lambda: arrived(x.at[:, :blocks * seg // heads], sent.at[TOKENS_Z]))
    pl.when(jnp.logical_not(inner))(lambda: arrived(x.at[:rows, :seg], sent.at[TOKENS_Z]))
    pl.when(inner)(lambda: arrived(x.at[:out_rows, :], sent.at[OUT_Z]))
    pl.when(jnp.logical_not(inner))(lambda: arrived(wo.at[0], sent.at[OUT_Z]))
    arrived(wown.at[:, :, :(heads - 1) * vdim], sent.at[WEIGHTS_Z])
    arrived(w.at[:(groups - 1) * heads * depth, :], sent.at[WEIGHTS_Y])
    arrived(x.at[:, :(heads - 1) * (parts - 1) * seg // heads], sent.at[SPREAD])
    arrived(kv.at[:heads * (groups - 1) * rows, :], sent.at[KEYS_Y])
    arrived(ho_out.at[:heads - 1], sent.at[HEADS_Z])
    arrived(ho.at[:groups - 1], sent.at[HEADS_Y])
    arrived(part_out, sent.at[PARTS])
    arrived(sum_out.at[:len(bits) - 1], sent.at[SUMS])
    arrived(part_out.at[:(groups - 1) * pairs], sent.at[RESULTS_Y])
    arrived(part_out, sent.at[RESULTS])


def solution(mesh):
    n, parts = mesh.shape["sp"], mesh.shape["tp"]

    def step(tokens, query_weight, key_weight, value_weight, out_weight, mix_lambda, head_gain):
        rows, width = tokens.shape
        heads = mix_lambda.shape[0]
        vdim = head_gain.shape[0]
        depth = query_weight.shape[0]
        groups = n // heads
        ocols = out_weight.shape[1]
        pairs = heads // 2
        pieces = groups * pairs
        nbits = parts.bit_length() - 1
        chunks = 2
        dma = pltpu.SemaphoreType.DMA
        bf16 = jnp.bfloat16
        limit = 32 * 1024 if n * rows <= 2048 else 60000
        operands = [pltpu.with_memory_space_constraint(operand, pltpu.HBM) for operand in (
            tokens, query_weight, key_weight, value_weight, out_weight, mix_lambda,
            head_gain.reshape(1, vdim),
        )]
        return pl.pallas_call(
            functools.partial(kernel, n, parts, heads, chunks),
            out_shape=pltpu.VMEM((rows, width), bf16),
            in_specs=[pl.BlockSpec(memory_space=pltpu.HBM)] * 7,
            out_specs=pl.BlockSpec(memory_space=pltpu.VMEM),
            scratch_shapes=[
                pltpu.VMEM((heads * rows, width), bf16),
                pltpu.VMEM((3, depth, heads * vdim), bf16),
                pltpu.VMEM((width, 3 * vdim), bf16),
                pltpu.VMEM((heads * rows, vdim), jnp.float32),
                pltpu.VMEM((heads * rows, vdim), bf16),
                pltpu.VMEM((n * rows, 2 * vdim), bf16),
                pltpu.VMEM((heads, heads * vdim, ocols), bf16),
                pltpu.VMEM((heads, rows, vdim), bf16),
                pltpu.VMEM((groups, heads, rows, vdim), bf16),
                pltpu.VMEM((pieces, rows, ocols), bf16),
                pltpu.VMEM((pieces, rows, ocols), bf16),
                pltpu.VMEM((nbits, pieces, rows, ocols), bf16),
                pltpu.VMEM((nbits, pieces, rows, ocols), bf16),
                pltpu.VMEM((n, rows, ocols), bf16),
                pltpu.VMEM((1, vdim), jnp.float32),
                pltpu.SMEM((heads,), jnp.float32),
                dma((10,)), dma((12,)),
                dma((heads, chunks)), dma((heads, parts // 2 - 1, chunks)), dma((heads,)),
                dma((heads, 3)), dma((3,)), dma((heads,)), dma((heads,)), dma((heads,)),
                dma((1,)), dma((pieces,)), dma((nbits - 1, pieces)), dma((groups, pairs)), dma((1,)),
            ],
            compiler_params=pltpu.CompilerParams(
                collective_id=0, has_side_effects=True, vmem_limit_bytes=limit * 1024
            ),
        )(*operands)

    placed = (
        P("sp", None),
        P("sp", "tp"),
        P("sp", "tp"),
        P("sp", "tp"),
        P("tp", "sp"),
        P("tp"),
        P(),
    )
    return jax.shard_map(step, mesh=mesh, in_specs=placed, out_specs=P("sp", None), check_vma=False)
```

profile of v0, /device:TPU:1, one launch (start us, length us, event | category | flops | bytes accessed | tf_op | source)
XLA Modules:
  0.0 63.2 jit_solution(5406931048103568026)
XLA Ops:
  0.0 62.4 %shard_map.73 = bf16[160,2048]{1,0:T(8,128)(2,1)S(1)} custom-call(bf16[160,2048]{1,0:T(8,128)(2,1)} %tok.1, bf16[256,512]{1,0:T(8,128)(2,1)} %wq.1, bf16[256,512]{1,0:T(8,128)(2,1)} %wk.1, bf16[256,512]{1,0:T(8,128)(2,1)} %wv.1, bf16[512,256]{1,0:T(8,128)(2,1)} %wo_in.1, f32[4]{0:T(128)} %lam_in.1, f32[1,128]{1,0:T(1,128)} %bitcast.1), custom_call_target="tpu_custom_call" | custom-call | tf_op jit(solution)/shard_map/pallas_call | solution.py:429
  62.4 0.8 %copy.9 = bf16[160,2048]{1,0:T(8,128)(2,1)} copy(bf16[160,2048]{1,0:T(8,128)(2,1)S(1)} %shard_map.73) | data formatting | bytes 1310720
where the time goes:
time: 64.3 us; the launch traced here: 63.2 us
  Pallas kernels  62.4 us (97%)
  local copies, waits for them, and re-layouts  0.84 us (1%)
    pallas_call x1, Pallas kernels, step(): pl.pallas_call(functools.partial(kernel, n, parts, heads, chunks), out_sh...  62.4 us

commit v1 on v0

--- a/solution.py
+++ b/solution.py
@@ -10,12 +10,13 @@
 MESH = pl.DeviceIdType.MESH
 Q, K, V = 0, 1, 2
 PLAN = (
-    "t0", "yv", "Wv1", "Wk3", "t10", "fv1", "t11", "Wv3", "Wv2", "Wk1", "yq", "Wq3", "yk", "fk3",
-    "t20", "fv2", "m11", "m20", "fv3", "m10", "Wk2", "fk1", "Wq1", "t21", "hv", "e1", "fq3", "m21",
-    "Wq2", "fk2", "fq1", "O", "t31", "hk", "t30", "b0", "fq2", "m31", "e2", "b2", "b1", "m30", "e3",
-    "b3", "gq", "o1", "hq", "dq", "a0", "a3", "a2", "a1", "r0", "r3", "o2", "r1", "r2", "P00",
-    "S00", "H", "P10", "S10", "o3", "P11", "X00", "S11", "X10", "P01", "S01", "X11", "F0", "F1",
-    "X01", "Z",
+    "yq", "yk", "yv", "t0", "Wk3", "Wv1", "Wv3", "t11", "Wv2", "t10", "Wq3", "Wq1", "Wk1", "t21",
+    "fv3", "fv1", "fv2", "m10", "t20", "m11", "fq1", "Wk2", "m20", "t31", "hv", "e1", "m21", "Wq2",
+    "fq3", "fk3", "fk1", "fk2", "O0", "O1", "t30", "fq2", "hk", "m31", "e2", "b0", "m30", "b1",
+    "e3", "gq", "b3", "o10", "o11", "hq", "b2", "dq", "a0", "a1", "a3", "a2", "o20", "o21", "r0",
+    "r1", "r2", "r3", "P00", "P01", "S00", "S01", "H", "P10", "P11", "S10", "S11", "X00", "X01",
+    "o30", "o31", "P12", "P13", "S12", "S13", "X10", "X11", "P02", "P03", "S02", "S03", "X12",
+    "X13", "X02", "X03", "F0", "F1", "F2", "F3", "Z",
 )
 
 
@@ -39,6 +40,8 @@
     low = lax.rem(t, 2)
     pairs = heads // 2
     chunk = rows // chunks
+    halves = wo.shape[0] // heads
+    hcols = ocols // halves
 
     def at_sp(index):
         return (index, t)
@@ -99,9 +102,12 @@
         loads["mine", i] = pltpu.make_async_copy(
             weights[i].at[:, ds(h, vdim)], w_at(s, i), local_sem.at[4 + i]
         )
-    loads["out"] = pltpu.make_async_copy(wo_in, wo.at[h], local_sem.at[7])
-    loads["lam"] = pltpu.make_async_copy(lam_in, lam, local_sem.at[8])
-    loads["gain"] = pltpu.make_async_copy(gain_in, gain, local_sem.at[9])
+    loads["lam"] = pltpu.make_async_copy(lam_in, lam, local_sem.at[7])
+    loads["gain"] = pltpu.make_async_copy(gain_in, gain, local_sem.at[8])
+    for c in range(halves):
+        loads["out", c] = pltpu.make_async_copy(
+            wo_in.at[:, pl.ds(c * hcols, hcols)], wo.at[h * halves + c], local_sem.at[9 + c]
+        )
     for copy in loads.values():
         copy.start()
 
@@ -231,17 +237,23 @@
         for safe, have, _ in reach(k):
             when(have, lambda safe=safe: body(safe))
 
-    def send_out_weight():
-        loaded("out")
+    def send_out_weight(c):
+        if c >= halves:
+            return
+        loaded(("out", c))
+        piece = h * halves + c
         for target, can in onward:
-            send(wo.at[h], wo.at[h], OUT_Z, wo_recv.at[h], target, can)
-
-    def relay_out_weight(k):
+            send(wo.at[piece], wo.at[piece], OUT_Z, wo_recv.at[piece], target, can)
+
+    def relay_out_weight(k, c):
+        if c >= halves:
+            return
         for safe, have, side in reach(k):
-            when(have, lambda safe=safe: arrived(wo.at[safe], wo_recv.at[safe]))
+            piece = safe * halves + c
+            when(have, lambda piece=piece: arrived(wo.at[piece], wo_recv.at[piece]))
             if k < heads - 1:
                 target, can = onward[side]
-                send(wo.at[safe], wo.at[safe], OUT_Z, wo_recv.at[safe], target,
+                send(wo.at[piece], wo.at[piece], OUT_Z, wo_recv.at[piece], target,
                      jnp.logical_and(have, can))
 
     lane = lax.broadcasted_iota(jnp.int32, (rows, vdim), 1)
@@ -304,34 +316,38 @@
     buddy = at_tp(flip(t, 1))
     members = [r] + others
 
-    def column_block(p, which):
-        return 2 * lax.rem(lax.div(h, 2) + p, pairs) + lax.rem(h + which, 2)
-
-    def which_rows(later):
-        return range(1, groups) if later else range(1)
-
-    def partial_product(e, p, which):
+    def column_block(pair, which):
+        return 2 * lax.rem(lax.div(h, 2) + pair, pairs) + lax.rem(h + which, 2)
+
+    def pieces_of(later, p):
+        pair, half = p // 2, p % 2
+        if half >= halves:
+            return []
+        return [
+            (e, pair, half, (e * pairs + pair) * halves + half)
+            for e in (range(1, groups) if later else range(1))
+        ]
+
+    def partial_product(e, pair, half, which):
         lhs = jnp.concatenate([ho[members[e], k] for k in range(heads)], axis=-1)
-        return jnp.dot(lhs, wo[column_block(p, which)], preferred_element_type=jnp.float32)
+        return jnp.dot(lhs, wo[column_block(pair, which) * halves + half],
+                       preferred_element_type=jnp.float32)
 
     def project_theirs(later, p):
-        for e in which_rows(later):
-            j = e * pairs + p
-            part_out[j] = partial_product(e, p, 1 - low).astype(jnp.bfloat16)
+        for e, pair, half, j in pieces_of(later, p):
+            part_out[j] = partial_product(e, pair, half, 1 - low).astype(jnp.bfloat16)
             send(part_out.at[j], part_in.at[j], PARTS, p_recv.at[j], buddy)
 
     def project_mine(later, p):
-        for e in which_rows(later):
-            j = e * pairs + p
-            own = partial_product(e, p, low)
+        for e, pair, half, j in pieces_of(later, p):
+            own = partial_product(e, pair, half, low)
             arrived(part_in.at[j], p_recv.at[j])
             sum_out[0, j] = (own + part_in[j].astype(jnp.float32)).astype(jnp.bfloat16)
             send(sum_out.at[0, j], sum_in.at[0, j], SUMS, s_recv.at[0, j], at_tp(flip(t, bits[1])))
 
     def add_up(later, p):
         last = len(bits) - 1
-        for e in which_rows(later):
-            j = e * pairs + p
+        for e, pair, half, j in pieces_of(later, p):
             for i in range(1, len(bits)):
                 arrived(sum_in.at[i - 1, j], s_recv.at[i - 1, j])
                 total = (
@@ -341,19 +357,19 @@
                     sum_out[i, j] = total
                     send(sum_out.at[i, j], sum_in.at[i, j], SUMS, s_recv.at[i, j],
                          at_tp(flip(t, bits[i + 1])))
-            column = column_block(p, low) * groups + r
+            place = (column_block(pair, low) * groups + r) * halves + half
             if e == 0:
-                staged[column] = total
-                send(staged.at[column], staged.at[column], RESULTS, d_recv.at[0], buddy)
+                staged[place] = total
+                send(staged.at[place], staged.at[place], RESULTS, d_recv.at[0], buddy)
             else:
                 sum_out[last, j] = total
-                send(sum_out.at[last, j], staged.at[column], RESULTS_Y, f_recv.at[r, p], peers[e - 1])
+                send(sum_out.at[last, j], staged.at[place], RESULTS_Y, f_recv.at[r, p], peers[e - 1])
 
     def finished(p):
-        for other in others:
-            column = column_block(p, low) * groups + other
-            arrived(staged.at[column], f_recv.at[other, p])
-            send(staged.at[column], staged.at[column], RESULTS, d_recv.at[0], buddy)
+        for e, pair, half, _ in pieces_of(True, p):
+            place = (column_block(pair, low) * groups + members[e]) * halves + half
+            arrived(staged.at[place], f_recv.at[members[e], p])
+            send(staged.at[place], staged.at[place], RESULTS, d_recv.at[0], buddy)
 
     def all_finished():
         arrived(part_in, d_recv.at[0])
@@ -370,8 +386,8 @@
         "b": lambda k: share_rows(int(k)),
         "g": lambda i: begin_queries(),
         "d": lambda i: finish_queries(),
-        "O": send_out_weight,
-        "o": lambda k: relay_out_weight(int(k)),
+        "O": lambda c: send_out_weight(int(c)),
+        "o": lambda k, c: relay_out_weight(int(k), int(c)),
         "a": lambda k: attend(int(k)),
         "r": lambda d: forward_heads(int(d)),
         "P": lambda e, p: project_theirs(int(e), int(p)),
@@ -384,15 +400,15 @@
     for name in PLAN:
         run[name[0]](*name[1:])
 
-    for column in range(n):
-        out[:, column * ocols:(column + 1) * ocols] = staged[column]
+    for place in range(n * halves):
+        out[:, place * hcols:(place + 1) * hcols] = staged[place]
     inner = jnp.logical_and(can_right, can_left)
     blocks = heads + 1
     out_rows = blocks * heads * vdim * ocols // width
     pl.when(inner)(lambda: arrived(x.at[:, :blocks * seg // heads], sent.at[TOKENS_Z]))
     pl.when(jnp.logical_not(inner))(lambda: arrived(x.at[:rows, :seg], sent.at[TOKENS_Z]))
     pl.when(inner)(lambda: arrived(x.at[:out_rows, :], sent.at[OUT_Z]))
-    pl.when(jnp.logical_not(inner))(lambda: arrived(wo.at[0], sent.at[OUT_Z]))
+    pl.when(jnp.logical_not(inner))(lambda: arrived(wo.at[:halves], sent.at[OUT_Z]))
     arrived(wown.at[:, :, :(heads - 1) * vdim], sent.at[WEIGHTS_Z])
     arrived(w.at[:(groups - 1) * heads * depth, :], sent.at[WEIGHTS_Y])
     arrived(x.at[:, :(heads - 1) * (parts - 1) * seg // heads], sent.at[SPREAD])
@@ -401,7 +417,7 @@
     arrived(ho.at[:groups - 1], sent.at[HEADS_Y])
     arrived(part_out, sent.at[PARTS])
     arrived(sum_out.at[:len(bits) - 1], sent.at[SUMS])
-    arrived(part_out.at[:(groups - 1) * pairs], sent.at[RESULTS_Y])
+    arrived(part_out.at[:(groups - 1) * pairs * halves], sent.at[RESULTS_Y])
     arrived(part_out, sent.at[RESULTS])
 
 
@@ -416,7 +432,9 @@
         groups = n // heads
         ocols = out_weight.shape[1]
         pairs = heads // 2
-        pieces = groups * pairs
+        halves = 2 if ocols % 256 == 0 else 1
+        hcols = ocols // halves
+        pieces = groups * pairs * halves
         nbits = parts.bit_length() - 1
         chunks = 2
         dma = pltpu.SemaphoreType.DMA
@@ -438,20 +456,20 @@
                 pltpu.VMEM((heads * rows, vdim), jnp.float32),
                 pltpu.VMEM((heads * rows, vdim), bf16),
                 pltpu.VMEM((n * rows, 2 * vdim), bf16),
-                pltpu.VMEM((heads, heads * vdim, ocols), bf16),
+                pltpu.VMEM((heads * halves, heads * vdim, hcols), bf16),
                 pltpu.VMEM((heads, rows, vdim), bf16),
                 pltpu.VMEM((groups, heads, rows, vdim), bf16),
-                pltpu.VMEM((pieces, rows, ocols), bf16),
-                pltpu.VMEM((pieces, rows, ocols), bf16),
-                pltpu.VMEM((nbits, pieces, rows, ocols), bf16),
-                pltpu.VMEM((nbits, pieces, rows, ocols), bf16),
-                pltpu.VMEM((n, rows, ocols), bf16),
+                pltpu.VMEM((pieces, rows, hcols), bf16),
+                pltpu.VMEM((pieces, rows, hcols), bf16),
+                pltpu.VMEM((nbits, pieces, rows, hcols), bf16),
+                pltpu.VMEM((nbits, pieces, rows, hcols), bf16),
+                pltpu.VMEM((n * halves, rows, hcols), bf16),
                 pltpu.VMEM((1, vdim), jnp.float32),
                 pltpu.SMEM((heads,), jnp.float32),
-                dma((10,)), dma((12,)),
+                dma((11,)), dma((12,)),
                 dma((heads, chunks)), dma((heads, parts // 2 - 1, chunks)), dma((heads,)),
-                dma((heads, 3)), dma((3,)), dma((heads,)), dma((heads,)), dma((heads,)),
-                dma((1,)), dma((pieces,)), dma((nbits - 1, pieces)), dma((groups, pairs)), dma((1,)),
+                dma((heads, 3)), dma((3,)), dma((heads,)), dma((heads * halves,)), dma((heads,)),
+                dma((1,)), dma((pieces,)), dma((nbits - 1, pieces)), dma((groups, pairs * 2)), dma((1,)),
             ],
             compiler_params=pltpu.CompilerParams(
                 collective_id=0, has_side_effects=True, vmem_limit_bytes=limit * 1024

time: 64.3 us -> 62.5 us (0.972); the launches traced: 63.2 us -> 62.3 us
  Pallas kernels: 62.4 us -> 61.5 us
    pallas_call x1, Pallas kernels: 62.4 us -> 61.5 us  [step(): pl.pallas_call(functools.partial(kernel, n, parts, heads, chunks), out_sh...]
where the time goes in v1:
time: 62.5 us; the launch traced here: 62.3 us
  Pallas kernels  61.5 us (98%)
  local copies, waits for them, and re-layouts  0.84 us (1%)
    pallas_call x1, Pallas kernels, step(): pl.pallas_call(functools.partial(kernel, n, parts, heads, chunks), out_sh...  61.5 us

profile of v1, /device:TPU:1, one launch (start us, length us, event | category | flops | bytes accessed | tf_op | source)
XLA Modules:
  0.0 62.3 jit_solution(6879341636722248256)
XLA Ops:
  0.0 61.5 %shard_map.73 = bf16[160,2048]{1,0:T(8,128)(2,1)S(1)} custom-call(bf16[160,2048]{1,0:T(8,128)(2,1)} %tok.1, bf16[256,512]{1,0:T(8,128)(2,1)} %wq.1, bf16[256,512]{1,0:T(8,128)(2,1)} %wk.1, bf16[256,512]{1,0:T(8,128)(2,1)} %wv.1, bf16[512,256]{1,0:T(8,128)(2,1)} %wo_in.1, f32[4]{0:T(128)} %lam_in.1, f32[1,128]{1,0:T(1,128)} %bitcast.1), custom_call_target="tpu_custom_call" | custom-call | tf_op jit(solution)/shard_map/pallas_call | solution.py:447
  61.5 0.8 %copy.9 = bf16[160,2048]{1,0:T(8,128)(2,1)} copy(bf16[160,2048]{1,0:T(8,128)(2,1)S(1)} %shard_map.73) | data formatting | bytes 1310720

commit v2 on v1

--- a/solution.py
+++ b/solution.py
@@ -13,10 +13,10 @@
     "yq", "yk", "yv", "t0", "Wk3", "Wv1", "Wv3", "t11", "Wv2", "t10", "Wq3", "Wq1", "Wk1", "t21",
     "fv3", "fv1", "fv2", "m10", "t20", "m11", "fq1", "Wk2", "m20", "t31", "hv", "e1", "m21", "Wq2",
     "fq3", "fk3", "fk1", "fk2", "O0", "O1", "t30", "fq2", "hk", "m31", "e2", "b0", "m30", "b1",
-    "e3", "gq", "b3", "o10", "o11", "hq", "b2", "dq", "a0", "a1", "a3", "a2", "o20", "o21", "r0",
+    "e3", "gq", "b3", "b2", "o10", "o11", "hq", "dq", "a0", "a1", "a3", "a2", "o20", "o21", "r0",
     "r1", "r2", "r3", "P00", "P01", "S00", "S01", "H", "P10", "P11", "S10", "S11", "X00", "X01",
-    "o30", "o31", "P12", "P13", "S12", "S13", "X10", "X11", "P02", "P03", "S02", "S03", "X12",
-    "X13", "X02", "X03", "F0", "F1", "F2", "F3", "Z",
+    "o30", "P12", "o31", "P13", "P02", "P03", "S12", "S13", "X10", "X11", "S02", "S03", "X12",
+    "X13", "F0", "F1", "X02", "X03", "F2", "F3", "Z",
 )
 
 
@@ -274,22 +274,38 @@
         q_rows = qb[k * rows:(k + 1) * rows, :]
         keys = kv[:extent, :vdim]
         values = kv[:extent, vdim:]
-        ahead = lax.broadcasted_iota(jnp.int32, (rows, extent), 1) - lax.broadcasted_iota(
-            jnp.int32, (rows, extent), 0
-        )
+        clear = k * groups * rows // 128 * 128
+        edge = extent - clear
+        row = lax.broadcasted_iota(jnp.int32, (2 * rows, edge), 0)
+        row = jnp.where(row >= rows, row - rows, row)
+        ahead = lax.broadcasted_iota(jnp.int32, (2 * rows, edge), 1) + clear - row
         visible = ahead <= (k * groups + r) * rows
-        maps = []
-        for c in range(2):
-            picked = jnp.where((lane >= vdim // 2) == (c == 1), q_rows, jnp.zeros_like(q_rows))
-            scores = lax.dot_general(
-                picked, keys, (((1,), (1,)), ((), ())), preferred_element_type=jnp.float32
+        zero = jnp.zeros_like(q_rows)
+        both = jnp.concatenate(
+            [jnp.where(lane < vdim // 2, q_rows, zero), jnp.where(lane >= vdim // 2, q_rows, zero)]
+        )
+        scores = lax.dot_general(
+            both, keys, (((1,), (1,)), ((), ())), preferred_element_type=jnp.float32
+        )
+        parts_of = [jnp.where(visible, scores[:, clear:], -1e30)]
+        if clear:
+            parts_of.insert(0, scores[:, :clear])
+        top = functools.reduce(
+            jnp.maximum, [jnp.max(part, axis=-1, keepdims=True) for part in parts_of]
+        )
+        total, mixed, start = None, None, 0
+        for part in parts_of:
+            e = jnp.exp2((part - top) * factor)
+            size = part.shape[-1]
+            term = jnp.sum(e, axis=-1, keepdims=True)
+            product = jnp.dot(
+                e.astype(jnp.bfloat16), values[start:start + size], preferred_element_type=jnp.float32
             )
-            scores = jnp.where(visible, scores, -1e30)
-            top = jnp.max(scores, axis=-1, keepdims=True)
-            e = jnp.exp2((scores - top) * factor)
-            total = jnp.sum(e, axis=-1, keepdims=True)
-            mixed = jnp.dot(e.astype(jnp.bfloat16), values, preferred_element_type=jnp.float32)
-            maps.append(mixed / total)
+            total = term if total is None else total + term
+            mixed = product if mixed is None else mixed + product
+            start += size
+        mixed = mixed / total
+        maps = (mixed[:rows], mixed[rows:])
         mixture = maps[0] - lam_here * maps[1]
         normalized = (
             mixture

time: 62.5 us -> 61.5 us (0.984)
  Pallas kernels: 61.5 us -> 60.5 us
    pallas_call x1, Pallas kernels: 61.5 us -> 60.5 us  [step(): pl.pallas_call(functools.partial(kernel, n, parts, heads, chunks), out_sh...]
where the time goes in v2:
time: 61.5 us; the launch traced here: 61.4 us
  Pallas kernels  60.5 us (98%)
  local copies, waits for them, and re-layouts  0.84 us (1%)
    pallas_call x1, Pallas kernels, step(): pl.pallas_call(functools.partial(kernel, n, parts, heads, chunks), out_sh...  60.5 us

profile of v2, /device:TPU:1, one launch (start us, length us, event | category | flops | bytes accessed | tf_op | source)
XLA Modules:
  0.0 61.4 jit_solution(17354747576715584057)
XLA Ops:
  0.0 60.5 %shard_map.73 = bf16[160,2048]{1,0:T(8,128)(2,1)S(1)} custom-call(bf16[160,2048]{1,0:T(8,128)(2,1)} %tok.1, bf16[256,512]{1,0:T(8,128)(2,1)} %wq.1, bf16[256,512]{1,0:T(8,128)(2,1)} %wk.1, bf16[256,512]{1,0:T(8,128)(2,1)} %wv.1, bf16[512,256]{1,0:T(8,128)(2,1)} %wo_in.1, f32[4]{0:T(128)} %lam_in.1, f32[1,128]{1,0:T(1,128)} %bitcast.1), custom_call_target="tpu_custom_call" | custom-call | tf_op jit(solution)/shard_map/pallas_call | solution.py:463
  60.5 0.8 %copy.9 = bf16[160,2048]{1,0:T(8,128)(2,1)} copy(bf16[160,2048]{1,0:T(8,128)(2,1)S(1)} %shard_map.73) | data formatting | bytes 1310720
